TPU v7x, 32 devices: a whole 2x2x4 slice. The times are simulated.
32 devices in a mesh: sp: 8 (over z, x), tp: 4 (over y, core).
Axes of the slice: x: 2, y: 2, z: 4, core: 2. Of those that a mesh axis runs over, the one named last changes fastest.
Arguments:
- resid: bfloat16 [6144, 2048], P(('sp', 'tp')), may hold values from -6 to 6
- queries: bfloat16 [6144, 1024], P('sp', 'tp'), may hold values from -160 to 160
- keys: bfloat16 [6144, 1024], P('sp', 'tp'), may hold values from -6 to 6
- values: bfloat16 [6144, 1024], P('sp', 'tp'), may hold values from -6 to 6
- cum_gate: float32 [6144, 16], P('sp', 'tp'), may hold values from -694 to 0, as said below
- out_weight: bfloat16 [1024, 2048], P('tp'), may hold values from -0.375 to 0.375
- norm_gain: float32 [2048], replicated, may hold values from 0.1 to 1.9
- gate_weight: bfloat16 [2048, 5504], P('sp', 'tp'), may hold values from -0.125 to 0.125
- up_weight: bfloat16 [2048, 5504], P('sp', 'tp'), may hold values from -0.125 to 0.125
- down_weight: bfloat16 [5504, 2048], P('tp', 'sp'), may hold values from -0.078125 to 0.078125
Outputs:
- layer_out: bfloat16 [6144, 2048], P(('sp', 'tp'))
Inputs may be any that keep to these rules, and one draw needn't show every extreme that they name: `cum_gate`: each column is non-increasing along positions and starts at or below zero.
All inputs are finite; a program needn't handle non-finite values.
Results may differ from a plain program's by a relative error of at most 0.01.
Values may be sent and summed in bfloat16 or wider, within the bound.
A program may use at most 256 MiB of HBM per device.

v0:
```python
import jax
import jax.numpy as jnp
from jax import lax
from jax.sharding import PartitionSpec as P

HEAD_DIM = 64


def rms_norm(mixed, norm_gain):
    scaled = mixed * lax.rsqrt(jnp.mean(mixed * mixed, axis=-1, keepdims=True) + 1e-06) * norm_gain
    return scaled.astype(jnp.bfloat16)


def rounded(term):
    return term.astype(jnp.bfloat16).astype(jnp.float32)


def local(
    resid,
    queries,
    keys,
    values,
    cum_gate,
    out_weight,
    norm_gain,
    gate_weight,
    up_weight,
    down_weight,
):
    rows = queries.shape[0]
    heads_here = cum_gate.shape[1]
    scale = HEAD_DIM ** (-0.5)
    proj_weight = lax.all_gather(out_weight, "tp", axis=0, tiled=True)
    first = lax.axis_index("sp") * rows
    gates_all = lax.all_gather(cum_gate, "sp", axis=0, tiled=True)
    query_heads = queries.reshape(rows, heads_here, HEAD_DIM)
    query_pos = first + jnp.arange(rows, dtype=jnp.int32)
    query_gate = cum_gate.T
    best = jnp.full((heads_here, rows), -1e30, jnp.float32)
    key_piece = lax.all_gather(keys, "sp", axis=0, tiled=True)
    value_piece = lax.all_gather(values, "sp", axis=0, tiled=True)
    count = key_piece.shape[0]
    key_heads = key_piece.reshape(count, heads_here, HEAD_DIM)
    value_heads = value_piece.reshape(count, heads_here, HEAD_DIM)
    key_gate = gates_all.T
    score = (
        jnp.einsum("qhd,khd->hqk", query_heads, key_heads, preferred_element_type=jnp.float32)
        * scale
    )
    score = score + query_gate[:, :, None] - key_gate[:, None, :]
    key_pos = jnp.arange(count, dtype=jnp.int32)
    score = jnp.where(key_pos[None, None, :] <= query_pos[None, :, None], score, -jnp.inf)
    new_best = jnp.maximum(best, jnp.max(score, axis=-1))
    weight = jnp.exp(score - new_best[:, :, None])
    total = jnp.sum(weight, axis=-1)
    numer = jnp.einsum(
        "hqk,khd->hqd", weight.astype(jnp.bfloat16), value_heads, preferred_element_type=jnp.float32
    )
    best, total, numer = (new_best, total, numer)
    attn = (
        (numer / total[:, :, None])
        .transpose(1, 0, 2)
        .reshape(rows, heads_here * HEAD_DIM)
        .astype(jnp.bfloat16)
    )
    groups = lax.axis_size("tp")
    share = rows // groups
    own_rows = lax.all_to_all(attn, "tp", split_axis=0, concat_axis=1, tiled=True)
    group_width = attn.shape[1]
    row_groups = own_rows.reshape(share, groups, group_width)
    weight_groups = proj_weight.reshape(groups, group_width, proj_weight.shape[1])
    terms = jnp.einsum(
        "rgc,gcd->grd", row_groups, weight_groups, preferred_element_type=jnp.float32
    )
    proj = jnp.sum(rounded(terms), axis=0)
    mixed = resid.astype(jnp.float32) + proj
    normed_all = lax.all_gather(rms_norm(mixed, norm_gain), "tp", axis=0, tiled=True)
    gate_sum = jnp.dot(
        normed_all,
        lax.all_gather(gate_weight, "sp", axis=0, tiled=True),
        preferred_element_type=jnp.float32,
    )
    up_sum = jnp.dot(
        normed_all,
        lax.all_gather(up_weight, "sp", axis=0, tiled=True),
        preferred_element_type=jnp.float32,
    )
    hidden = (jax.nn.silu(gate_sum) * up_sum).astype(jnp.bfloat16)
    ffn_part = jnp.dot(
        hidden,
        lax.all_gather(down_weight, "sp", axis=1, tiled=True),
        preferred_element_type=jnp.float32,
    )
    ffn = lax.psum_scatter(
        rounded(ffn_part).astype(jnp.bfloat16), "tp", scatter_dimension=0, tiled=True
    ).astype(jnp.float32)
    return (mixed + 0.5 * ffn).astype(jnp.bfloat16)


def solution(mesh):
    in_specs = (
        P(("sp", "tp"), None),
        P("sp", "tp"),
        P("sp", "tp"),
        P("sp", "tp"),
        P("sp", "tp"),
        P("tp", None),
        P(),
        P("sp", "tp"),
        P("sp", "tp"),
        P("tp", "sp"),
    )
    out_specs = P(("sp", "tp"), None)
    return jax.shard_map(local, mesh=mesh, in_specs=in_specs, out_specs=out_specs, check_vma=False)
```

profile of v0, /device:TPU:0, one launch (start us, length us, event | category | flops | bytes accessed | tf_op | source)
XLA Modules:
  0.0 547.6 jit_solution(295551948475313620)
XLA Ops:
  6.5 0.0 copy-start.2
  6.5 0.0 copy-start.1
  6.5 0.0 all-gather.8.cloned.1.call-start
  6.5 0.7 all-gather.8.cloned.1.call-update
  7.3 0.0 all-gather.10.cloned.1.call-start
  7.3 0.7 all-gather.10.cloned.1.call-update
  8.0 0.0 all-gather.12.cloned.1.call-start
  8.1 0.7 all-gather.12.cloned.1.call-update
  8.7 0.0 all-gather.16.cloned.1.call-start
  8.8 0.5 all-gather.16.cloned.1.call-update
  9.3 0.0 all-gather.14.cloned.1.call-start
  9.4 5.7 %iota_compare_fusion = pred[768,6144]{1,0:T(8,128)(4,1)} fusion(s32[768]{0:T(1024)S(1)} %iota_add_fusion), kind=kLoop, calls=%fused_computation.7 | loop fusion | flops 4718592 | bytes 4721664 | tf_op jit(solution)/shard_map/le | solution.py:52
  15.1 0.0 copy-done.2
  15.1 32.9 %all_gather.25 = f32[6144,4]{0,1:T(4,128)S(1)} all-gather(f32[768,4]{0,1:T(4,128)S(1)} %copy-done.2), channel_id=1, replica_groups=mesh['sp'=8,'tp'=4] {'sp'}, dimensions={0}, use_global_device_ids=true | all-gather | bytes 110592 | tf_op jit(solution)/shard_map/all_gather | solution.py:35
  47.9 0.0 copy-done.1
  48.0 0.9 copy.15
  48.9 23.7 %all-gather.8.cloned.1.call-done = bf16[6144,256]{1,0:T(8,128)(2,1)} async-done(((bf16[768,256]{1,0:T(8,128)(2,1)}), bf16[6144,256]{1,0:T(8,128)(2,1)}) %all-gather.8.cloned.1.call-update) | async-done | bytes 3145744 | tf_op jit(solution)/shard_map/all_gather | solution.py:40
  72.6 3.3 copy.16
  76.0 31.1 %fusion.2 = (f32[4,768]{1,0:T(4,128)S(1)}, f32[4,768,6144]{2,1,0:T(8,128)}) fusion(f32[4,6144]{1,0:T(4,128)S(1)} %bitcast.30, f32[4,768]{1,0:T(4,128)S(1)} %bitcast.34, pred[768,6144]{1,0:T(8,128)(4,1)} %iota_compare_fusion, bf16[768,4,64]{0,2,1:T(8,128)(2,1)} %bitcast.33, bf16[6144,4,64]{0,2,1:T(8,128)(2,1)S(1)} %bitcast.29), kind=kOutput, calls=%fused_computation.4 | convolution fusion | flops 2510287872 | bytes 83877888 | tf_op jit(solution)/shard_map/qhd,khd->hqk/dot_general | solution.py:47
  107.1 26.6 %all-gather.10.cloned.1.call-done = bf16[6144,256]{1,0:T(8,128)(2,1)} async-done(((bf16[768,256]{1,0:T(8,128)(2,1)}), bf16[6144,256]{1,0:T(8,128)(2,1)}) %all-gather.10.cloned.1.call-update) | async-done | bytes 3145744 | tf_op jit(solution)/shard_map/all_gather | solution.py:41
  133.7 3.2 copy.17
  136.9 30.4 %fusion = f32[4,768]{1,0:T(4,128)S(1)} fusion(f32[4,768,6144]{2,1,0:T(8,128)} %get-tuple-element.6, f32[4,768]{1,0:T(4,128)S(1)} %broadcast_maximum_fusion, f32[4,6144]{1,0:T(4,128)S(1)} %bitcast.31, f32[4,768]{1,0:T(4,128)S(1)} %bitcast.35, pred[768,6144]{1,0:T(8,128)(4,1)} %iota_compare_fusion), kind=kLoop, calls=%fused_computation.2 | loop fusion | flops 113243136 | bytes 80351232 | tf_op jit(solution)/shard_map/reduce_sum | solution.py:55
  167.3 31.7 %fusion.12 = bf16[768,4,64]{0,2,1:T(8,128)(2,1)} fusion(bf16[6144,4,64]{0,2,1:T(8,128)(2,1)S(1)} %bitcast.28, f32[4,768,6144]{2,1,0:T(8,128)} %get-tuple-element.6, f32[4,768]{1,0:T(4,128)S(1)} %broadcast_maximum_fusion, f32[4,6144]{1,0:T(4,128)S(1)} %bitcast.32, f32[4,768]{1,0:T(4,128)S(1)} %bitcast.36, pred[768,6144]{1,0:T(8,128)(4,1)} %iota_compare_fusion, ...), kind=kOutput, calls=%fused_computation.18 | convolution fusion | flops 2529558528 | bytes 83890176 | tf_op jit(solution)/shard_map/hqk,khd->hqd/dot_general | solution.py:56
  198.9 1.5 convert_element_type.39
  200.4 0.3 copy.18
  200.8 0.0 copy-start
  200.8 9.9 %all_to_all.13 = bf16[4,192,256]{2,1,0:T(8,128)(2,1)S(1)} all-to-all(bf16[4,192,256]{2,1,0:T(8,128)(2,1)S(1)} %copy.18), channel_id=1, replica_groups=mesh['sp'=8,'tp'=4] {'tp'}, dimensions={0} | all-to-all | bytes 786432 | tf_op jit(solution)/shard_map/all_to_all | solution.py:68
  210.7 0.0 all-gather.12.cloned.1.call-done
  210.7 3.5 convert_reduce_fusion
  214.2 0.0 copy-done
  214.2 0.3 multiply_reduce_fusion
  214.5 0.0 copy-done.3
  214.5 1.1 multiply_convert_fusion.1
  215.6 0.0 all-gather.14.cloned.1.call-update
  215.7 0.0 all-gather.18.cloned.1.call-start
  215.7 0.5 all-gather.18.cloned.1.call-update
  216.2 0.0 all-gather.20.cloned.1.call-start
  216.3 0.7 all-gather.20.cloned.1.call-update
  217.0 0.3 reduce-scatter.2.cloned.1.call-start
  217.2 44.6 %all-gather.16.cloned.1.call-done = bf16[2048,1376]{0,1:T(8,128)(2,1)} async-done(((bf16[256,1376]{0,1:T(8,128)(2,1)}), bf16[2048,1376]{0,1:T(8,128)(2,1)}) %all-gather.16.cloned.1.call-update) | async-done | bytes 5636112 | tf_op jit(solution)/shard_map/all_gather | solution.py:80
  261.9 28.1 %all-gather.14.cloned.1.call-done = bf16[768,2048]{1,0:T(8,128)(2,1)} async-done(((bf16[192,2048]{1,0:T(8,128)(2,1)}), bf16[768,2048]{1,0:T(8,128)(2,1)}) %all-gather.14.cloned.1.call-update) | async-done | bytes 3145744 | tf_op jit(solution)/shard_map/all_gather | solution.py:77
  290.0 10.2 %fusion.19 = f32[768,1376]{0,1:T(8,128)} fusion(bf16[768,2048]{1,0:T(8,128)(2,1)} %all-gather.14.cloned.1.call-done, bf16[2048,1376]{0,1:T(8,128)(2,1)} %all-gather.16.cloned.1.call-done), kind=kOutput, calls=%fused_computation.26 | convolution fusion | flops 4328521728 | bytes 13008896 | tf_op jit(solution)/shard_map/dot_general | solution.py:78
  300.2 83.3 %all-gather.18.cloned.1.call-done = bf16[2048,1376]{0,1:T(8,128)(2,1)} async-done(((bf16[256,1376]{0,1:T(8,128)(2,1)}), bf16[2048,1376]{0,1:T(8,128)(2,1)}) %all-gather.18.cloned.1.call-update) | async-done | bytes 5636112 | tf_op jit(solution)/shard_map/all_gather | solution.py:85
  383.5 91.8 %all-gather.20.cloned.1.call-done = bf16[1376,2048]{1,0:T(8,128)(2,1)} async-done(((bf16[1376,256]{1,0:T(8,128)(2,1)}), bf16[1376,2048]{1,0:T(8,128)(2,1)}) %all-gather.20.cloned.1.call-update) | async-done | bytes 5636112 | tf_op jit(solution)/shard_map/all_gather | solution.py:91
  475.3 26.5 %convolution_convert_fusion.1 = bf16[768,2048]{1,0:T(8,128)(2,1)} fusion(bf16[1376,2048]{1,0:T(8,128)(2,1)} %all-gather.20.cloned.1.call-done, f32[768,1376]{0,1:T(8,128)} %fusion.19, bf16[768,2048]{1,0:T(8,128)(2,1)} %all-gather.14.cloned.1.call-done, bf16[2048,1376]{0,1:T(8,128)(2,1)} %all-gather.18.cloned.1.call-done), kind=kOutput, calls=%fused_computation.11 | convolution fusion | flops 8664956928 | bytes 21790720 | tf_op jit(solution)/shard_map/dot_general | solution.py:89
  501.8 0.0 reduce-scatter.2.cloned.1.call-update
  501.8 36.2 %reduce-scatter.2.cloned.1.call-done = bf16[192,2048]{1,0:T(8,128)(2,1)} async-done(((bf16[768,2048]{1,0:T(8,128)(2,1)}), bf16[192,2048]{1,0:T(8,128)(2,1)}) %reduce-scatter.2.cloned.1.call-update) | async-done | bytes 786448 | tf_op jit(solution)/shard_map/reduce_scatter | solution.py:94
  538.0 2.3 add_convert_fusion
  (4 shorter events, 0.0 us)
Async XLA Ops:
  6.5 8.6 %copy-start.2 = (f32[768,4]{0,1:T(4,128)S(1)}, f32[768,4]{0,1:T(4,128)}, u32[]{:S(2)}) copy-start(f32[768,4]{0,1:T(4,128)} %param.14) | copy-start | bytes 36868
  6.5 41.4 %copy-start.1 = (bf16[768,256]{1,0:T(8,128)(2,1)S(1)}, bf16[768,256]{1,0:T(8,128)(2,1)}, u32[]{:S(2)}) copy-start(bf16[768,256]{1,0:T(8,128)(2,1)} %param.11) | copy-start | bytes 1179652
  6.5 66.1 %all-gather.8.cloned.1.call-start = ((), (), s32[]{:S(2)}) async-start(), calls=%async_computation.2 | async-start | bytes 3538944 | tf_op jit(solution)/shard_map/all_gather | solution.py:40
  7.3 126.4 %all-gather.10.cloned.1.call-start = ((), (), s32[]{:S(2)}) async-start(), calls=%async_computation.3 | async-start | bytes 3538944 | tf_op jit(solution)/shard_map/all_gather | solution.py:41
  8.0 202.7 %all-gather.12.cloned.1.call-start = ((), (), s32[]{:S(2)}) async-start(), calls=%async_computation.4 | async-start | bytes 5242880 | tf_op jit(solution)/shard_map/all_gather | solution.py:33
  8.7 253.1 %all-gather.16.cloned.1.call-start = ((), (), s32[]{:S(2)}) async-start(), calls=%async_computation.6 | async-start | bytes 6340608 | tf_op jit(solution)/shard_map/all_gather | solution.py:80
  9.3 280.7 %all-gather.14.cloned.1.call-start = ((), (), s32[]{:S(2)}) async-start(), calls=%async_computation.5 | async-start | bytes 3932160 | tf_op jit(solution)/shard_map/all_gather | solution.py:77
  200.8 13.4 %copy-start = (bf16[192,2048]{1,0:T(8,128)(2,1)S(1)}, bf16[192,2048]{1,0:T(8,128)(2,1)}, u32[]{:S(2)}) copy-start(bf16[192,2048]{1,0:T(8,128)(2,1)} %param.10) | copy-start | bytes 2359300
  210.7 3.8 copy-start.3
  215.7 167.8 %all-gather.18.cloned.1.call-start = ((), (), s32[]{:S(2)}) async-start(), calls=%async_computation.7 | async-start | bytes 6340608 | tf_op jit(solution)/shard_map/all_gather | solution.py:85
  216.2 259.1 %all-gather.20.cloned.1.call-start = ((), (), s32[]{:S(2)}) async-start(), calls=%async_computation.8 | async-start | bytes 6340608 | tf_op jit(solution)/shard_map/all_gather | solution.py:91
  217.0 321.0 %reduce-scatter.2.cloned.1.call-start = ((), (), s32[]{:S(2)}) async-start(), calls=%async_computation.9 | async-start | bytes 3932160 | tf_op jit(solution)/shard_map/reduce_scatter | solution.py:94
Sparse Core Ops, SparseCore 0:
  9.5 63.0 all-gather.7
  74.8 58.8 all-gather.9
  135.3 33.1 all-gather.11
  170.3 91.5 all-gather.15
  263.3 26.6 all-gather.13
  291.9 91.5 all-gather.17
  385.5 89.7 all-gather.19
  501.9 36.0 reduce-scatter.1
where the time goes:
time: 552 us; the launch traced here: 548 us
  waiting for transfers between devices  338 us (61%)
  matrix products  103 us (19%)
  blocking collectives  42.8 us (8%)
  other arithmetic  39.9 us (7%)
  between operations  14 us (3%)
  local copies, waits for them, and re-layouts  9.28 us (2%)
    all_gather x1, waiting for transfers between devices, local(): lax.all_gather(down_weight, 'sp', axis=1, tiled=True)  91.8 us
    all_gather x1, waiting for transfers between devices, local(): lax.all_gather(up_weight, 'sp', axis=0, tiled=True)  83.3 us
    all_gather x1, waiting for transfers between devices, local(): lax.all_gather(gate_weight, 'sp', axis=0, tiled=True)  44.6 us
    reduce_scatter x1, waiting for transfers between devices, local(): lax.psum_scatter(rounded(ffn_part).astype(jnp.bfloat16), 'tp', scatter_di...  36.2 us
    all_gather x1, blocking collectives, local(): gates_all = lax.all_gather(cum_gate, 'sp', axis=0, tiled=True)  32.9 us
    dot_general x1, matrix products, local(): jnp.einsum('hqk,khd->hqd', weight.astype(jnp.bfloat16), value_heads, pref...  31.7 us
    dot_general x1, matrix products, local(): jnp.einsum('qhd,khd->hqk', query_heads, key_heads, preferred_element_type...  31.1 us
    reduce_sum x1, other arithmetic, local(): total = jnp.sum(weight, axis=-1)  30.4 us
  transfers between devices with their start and end apart: 8, of which 7 were waited for; matrix products, arithmetic and copies ran while one was open for 23% of the time, Pallas kernels for 0%

commit v1 on v0

v1 whole, which is shorter than its diff:
```python
import functools

import jax
import jax.numpy as jnp
from jax import lax
from jax.experimental import pallas as pl
from jax.experimental.pallas import tpu as pltpu
from jax.sharding import Mesh
from jax.sharding import PartitionSpec as P

HEAD_DIM = 64
LOG2E = 1.4426950408889634


def rms_norm(mixed, norm_gain):
    scaled = mixed * lax.rsqrt(jnp.mean(mixed * mixed, axis=-1, keepdims=True) + 1e-06) * norm_gain
    return scaled.astype(jnp.bfloat16)


def rounded(term):
    return term.astype(jnp.bfloat16).astype(jnp.float32)


def flash_kernel(rows, q_block, shard_ref, q_ref, k_ref, v_ref, gate_q_ref, gate_k_ref, out_ref):
    pair = pl.program_id(0)
    block = pl.program_id(1)
    shard = shard_ref[0]
    q = q_ref[...]
    lane = lax.broadcasted_iota(jnp.int32, (q_block, 2 * HEAD_DIM), 1)
    low = lane < HEAD_DIM
    zero = jnp.zeros_like(q)
    q_heads = (jnp.where(low, q, zero), jnp.where(low, zero, q))
    gate_q = gate_q_ref[...]
    gate_lane = lax.broadcasted_iota(jnp.int32, gate_q.shape, 1)
    gates = tuple(
        jnp.sum(jnp.where(gate_lane == 2 * pair + h, gate_q, 0.0), axis=1, keepdims=True) * LOG2E
        for h in range(2)
    )
    scale = HEAD_DIM ** (-0.5) * LOG2E

    def step(j, state, masked):
        best, total, numer = state
        start = pl.multiple_of(j * rows, rows)
        k = k_ref[pl.ds(start, rows), :]
        v = v_ref[pl.ds(start, rows), :]
        new_best, new_total, parts, decay = [], [], [], []
        for h in range(2):
            s = lax.dot_general(
                q_heads[h], k, (((1,), (1,)), ((), ())), preferred_element_type=jnp.float32
            )
            gate_k = gate_k_ref[j, 0, h : h + 1, :] * LOG2E
            s = s * scale + (gates[h] - gate_k)
            if masked:
                row = lax.broadcasted_iota(jnp.int32, s.shape, 0) + block * q_block
                col = lax.broadcasted_iota(jnp.int32, s.shape, 1)
                s = jnp.where(col <= row, s, -1e30)
            top = jnp.maximum(best[h], jnp.max(s, axis=1, keepdims=True))
            keep = jnp.exp2(best[h] - top)
            w = jnp.exp2(s - top)
            new_best.append(top)
            new_total.append(total[h] * keep + jnp.sum(w, axis=1, keepdims=True))
            parts.append(
                lax.dot_general(
                    w.astype(jnp.bfloat16), v, (((1,), (0,)), ((), ())),
                    preferred_element_type=jnp.float32,
                )
            )
            decay.append(keep)
        numer = numer * jnp.where(low, decay[0], decay[1]) + jnp.where(low, parts[0], parts[1])
        return tuple(new_best), tuple(new_total), numer

    column = jnp.zeros((q_block, 1), jnp.float32)
    state = (
        (column - 1e30, column - 1e30),
        (column, column),
        jnp.zeros((q_block, 2 * HEAD_DIM), jnp.float32),
    )
    state = step(shard, state, True)
    state = lax.fori_loop(0, shard, lambda j, s: step(j, s, False), state)
    _, total, numer = state
    out_ref[...] = (numer / jnp.where(low, total[0], total[1])).astype(jnp.bfloat16)


def flash(shard, queries, kv_all, cum_gate, gates_all):
    rows, width = queries.shape
    pairs = width // (2 * HEAD_DIM)
    count = kv_all.shape[0]
    shards = count // rows
    heads = cum_gate.shape[1]
    q_block = 256 if rows % 256 == 0 else rows
    two = 2 * HEAD_DIM
    gates_all = gates_all.reshape(shards, pairs, 2, rows)
    return pl.pallas_call(
        functools.partial(flash_kernel, rows, q_block),
        grid=(pairs, rows // q_block),
        in_specs=[
            pl.BlockSpec(memory_space=pltpu.SMEM),
            pl.BlockSpec((q_block, two), lambda p, i: (i, p)),
            pl.BlockSpec((count, two), lambda p, i: (0, p)),
            pl.BlockSpec((count, two), lambda p, i: (0, pairs + p)),
            pl.BlockSpec((q_block, heads), lambda p, i: (i, 0)),
            pl.BlockSpec((shards, 1, 2, rows), lambda p, i: (0, p, 0, 0)),
        ],
        out_specs=pl.BlockSpec((q_block, two), lambda p, i: (i, p)),
        out_shape=jax.ShapeDtypeStruct((rows, width), jnp.bfloat16),
        compiler_params=pltpu.CompilerParams(vmem_limit_bytes=40 * 2**20),
        cost_estimate=pl.CostEstimate(
            flops=8 * rows * count * width,
            bytes_accessed=4 * count * width,
            transcendentals=rows * count * width // HEAD_DIM,
        ),
    )(shard.reshape(1), queries, kv_all, kv_all, cum_gate, gates_all)


def shift(value, axis, size, step):
    return lax.ppermute(value, axis, [(i, (i + step) % size) for i in range(size)])


def exchange(weight, split, joined, size):
    here = lax.axis_index("x")
    width = weight.shape[split] // size
    pieces = []
    for step in range(size):
        target = lax.rem(here + step, size)
        piece = lax.dynamic_slice_in_dim(weight, target * width, width, split)
        pieces.append(piece if step == 0 else shift(piece, "x", size, step))
    if size == 1:
        return pieces[0]
    if size == 2:
        first = here == 0
        return jnp.concatenate(
            [jnp.where(first, pieces[0], pieces[1]), jnp.where(first, pieces[1], pieces[0])], joined
        )
    length = weight.shape[joined]
    shape = list(pieces[0].shape)
    shape[joined] = length * size
    whole = jnp.zeros(shape, weight.dtype)
    for step in range(size):
        source = lax.rem(here - step + size, size)
        whole = lax.dynamic_update_slice_in_dim(whole, pieces[step], source * length, joined)
    return whole


def local(
    resid,
    queries,
    keys,
    values,
    cum_gate,
    out_weight,
    norm_gain,
    gate_weight,
    up_weight,
    down_weight,
):
    rows = queries.shape[0]
    along_x = lax.axis_size("x")
    groups = lax.axis_size("tp")
    shard = lax.axis_index("z") * along_x + lax.axis_index("x")
    gates_all = lax.all_gather(cum_gate.T, ("z", "x"), axis=0)
    kv_all = lax.all_gather(jnp.concatenate([keys, values], axis=1), ("z", "x"), axis=0, tiled=True)
    proj_weights = [out_weight] + [shift(out_weight, "tp", groups, d) for d in range(1, groups)]
    gate_cols = exchange(gate_weight, 1, 0, along_x)
    up_cols = exchange(up_weight, 1, 0, along_x)
    down_rows = exchange(down_weight, 0, 1, along_x)
    gate_full = lax.all_gather(gate_cols, "z", axis=0, tiled=True)
    up_full = lax.all_gather(up_cols, "z", axis=0, tiled=True)
    down_full = lax.all_gather(down_rows, "z", axis=1, tiled=True)

    attn = flash(shard.astype(jnp.int32), queries, kv_all, cum_gate, gates_all)

    own_rows = lax.all_to_all(attn, "tp", split_axis=0, concat_axis=1, tiled=True)
    width = attn.shape[1]
    here = lax.axis_index("tp")
    mixed = resid.astype(jnp.float32)
    for d in range(groups):
        group = lax.rem(here - d + groups, groups)
        part = lax.dynamic_slice_in_dim(own_rows, group * width, width, 1)
        mixed = mixed + rounded(
            jnp.dot(part, proj_weights[d], preferred_element_type=jnp.float32)
        )
    normed_all = lax.all_gather(rms_norm(mixed, norm_gain), ("x", "tp"), axis=0, tiled=True)
    gate_sum = jnp.dot(normed_all, gate_full, preferred_element_type=jnp.float32)
    up_sum = jnp.dot(normed_all, up_full, preferred_element_type=jnp.float32)
    hidden = (jax.nn.silu(gate_sum) * up_sum).astype(jnp.bfloat16)
    ffn_part = jnp.dot(hidden, down_full, preferred_element_type=jnp.float32)
    ffn = lax.psum_scatter(
        ffn_part.astype(jnp.bfloat16), ("x", "tp"), scatter_dimension=0, tiled=True
    ).astype(jnp.float32)
    return (mixed + 0.5 * ffn).astype(jnp.bfloat16)


def solution(mesh):
    along_sp = mesh.shape["sp"]
    along_x = 2 if along_sp % 2 == 0 else 1
    grid = Mesh(
        mesh.devices.reshape(along_sp // along_x, along_x, mesh.shape["tp"]), ("z", "x", "tp")
    )
    sp = ("z", "x")
    in_specs = (
        P(("z", "x", "tp"), None),
        P(sp, "tp"),
        P(sp, "tp"),
        P(sp, "tp"),
        P(sp, "tp"),
        P("tp", None),
        P(),
        P(sp, "tp"),
        P(sp, "tp"),
        P("tp", sp),
    )
    out_specs = P(("z", "x", "tp"), None)
    return jax.shard_map(local, mesh=grid, in_specs=in_specs, out_specs=out_specs, check_vma=False)
```

time: 552 us -> 454 us (0.82)
  matrix products: 103 us -> 33.1 us
  other arithmetic: 39.9 us -> 8.64 us
  starting transfers between devices: 0.48 us -> 18.8 us
  blocking collectives: 42.8 us -> 31.9 us
  Pallas kernels: 0 us -> 9.68 us
    dot_general x5 -> x6, matrix products: 103 us -> 33.1 us  [the longest x1 18.8 us: local(): ffn_part = jnp.dot(hidden, down_full, preferred_element_type=jnp.float32)]
    all_gather x7 -> x5, waiting for transfers between devices: 298 us -> 238 us  [the longest x1 73.5 us: local(): lax.all_gather(rms_norm(mixed, norm_gain), ('x', 'tp'), axis=0, tiled=True)]
    reduce_sum x2 -> x0, other arithmetic: 30.7 us -> none  [the longest x1 30.4 us: local(): total = jnp.sum(weight, axis=-1)]
    ppermute x0 -> x6, waiting for transfers between devices: none -> 28 us  [shift(): lax.ppermute(value, axis, [(i, (i + step) % size) for i in range(size)])]
    reduce_scatter x1, waiting for transfers between devices: 36.2 us -> 60.6 us  [local(): lax.psum_scatter(ffn_part.astype(jnp.bfloat16), ('x', 'tp'), scatter_dime...]
    ppermute x0 -> x6, starting transfers between devices: none -> 15 us  [shift(): lax.ppermute(value, axis, [(i, (i + step) % size) for i in range(size)])]
    all_to_all x1 -> x0, blocking collectives: 9.94 us -> none  [local(): lax.all_to_all(attn, 'tp', split_axis=0, concat_axis=1, tiled=True)]
    pallas_call x0 -> x1, Pallas kernels: none -> 9.68 us  [flash(): pl.pallas_call(functools.partial(flash_kernel, rows, q_block), grid=(pair...]
  transfers between devices with their start and end apart: 8 -> 13, of which waited for: 7 -> 10; matrix products, arithmetic and copies ran while one was open for 23% -> 4% of each run, Pallas kernels for 0% -> 2%
where the time goes in v1:
time: 454 us
  waiting for transfers between devices  334 us (74%)
  matrix products  33.1 us (7%)
  blocking collectives  31.9 us (7%)
  starting transfers between devices  18.8 us (4%)
  between operations  13.7 us (3%)
  Pallas kernels  9.68 us (2%)
  other arithmetic  8.64 us (2%)
    all_gather x1, waiting for transfers between devices, local(): lax.all_gather(rms_norm(mixed, norm_gain), ('x', 'tp'), axis=0, tiled=True)  73.5 us
    reduce_scatter x1, waiting for transfers between devices, local(): lax.psum_scatter(ffn_part.astype(jnp.bfloat16), ('x', 'tp'), scatter_dime...  60.6 us
    all_gather x1, waiting for transfers between devices, local(): up_full = lax.all_gather(up_cols, 'z', axis=0, tiled=True)  58.2 us
    all_gather x1, waiting for transfers between devices, local(): lax.all_gather(jnp.concatenate([keys, values], axis=1), ('z', 'x'), axis=...  56.6 us
    all_gather x1, waiting for transfers between devices, local(): down_full = lax.all_gather(down_rows, 'z', axis=1, tiled=True)  49.4 us
    all_gather x1, blocking collectives, local(): gates_all = lax.all_gather(cum_gate.T, ('z', 'x'), axis=0)  31.9 us
    ppermute x6, waiting for transfers between devices, shift(): lax.ppermute(value, axis, [(i, (i + step) % size) for i in range(size)])  28 us
    dot_general x1, matrix products, local(): ffn_part = jnp.dot(hidden, down_full, preferred_element_type=jnp.float32)  18.8 us
  transfers between devices with their start and end apart: 13, of which 10 were waited for; matrix products, arithmetic and copies ran while one was open for 4% of the time, Pallas kernels for 2%

profile of v1, /device:TPU:0, one launch (start us, length us, event | category | flops | bytes accessed | tf_op | source)
XLA Modules:
  0.0 453.7 jit_solution(16537196910402588736)
XLA Ops:
  6.5 2.1 pad_maximum_fusion
  8.7 0.0 all-gather.8.cloned.1.call-update
  8.7 0.0 all-gather.12.cloned.1.call-start
  8.8 3.0 collective-permute-start.3
  11.8 8.2 %collective-permute-done.3 = bf16[256,688]{0,1:T(8,128)(2,1)S(1)} collective-permute-done((bf16[256,688]{0,1:T(8,128)(2,1)S(1)}, bf16[256,688]{0,1:T(8,128)(2,1)S(1)}, u32[]{:S(2)}, u32[]{:S(2)}) %collective-permute-start.3) | collective-permute-done | bytes 352288 | tf_op jit(solution)/shard_map/ppermute | solution.py:116
  20.1 0.2 broadcast_select_fusion.5
  20.2 0.9 pad_maximum_fusion.1
  21.2 0.0 all-gather.12.cloned.1.call-update
  21.2 0.4 collective-permute-start.2
  21.6 1.5 collective-permute-start.1
  23.1 0.2 copy.14.gate_q_ref
  23.3 31.9 %all-gather.1 = f32[8,4,768]{2,1,0:T(4,128)S(1)} all-gather(f32[1,4,768]{2,1,0:T(4,128)S(1)} %bitcast.22), channel_id=2, replica_groups=mesh['z'=4,'x'=2,'tp'=4] {'z','x'}, dimensions={0}, use_global_device_ids=true | all-gather | bytes 110592 | tf_op jit(solution)/shard_map/all_gather | solution.py:160
  55.2 0.1 reshape.19.gate_k_ref
  55.3 56.6 %all-gather.8.cloned.1.call-done.k_ref.v_ref = bf16[6144,512]{1,0:T(8,128)(2,1)} async-done(((bf16[768,512]{1,0:T(8,128)(2,1)}), bf16[6144,512]{1,0:T(8,128)(2,1)}) %all-gather.8.cloned.1.call-update) | async-done | bytes 6291472 | tf_op jit(solution)/shard_map/all_gather | solution.py:161
  111.8 2.8 copy-done
  114.6 9.7 %shard_map.100 = bf16[768,256]{1,0:T(8,128)(2,1)} custom-call(s32[1]{0:T(128)} %bitcast.shard_ref, bf16[768,256]{1,0:T(8,128)(2,1)S(1)} %copy-done.1, bf16[6144,512]{1,0:T(8,128)(2,1)S(1)} %copy-done, bf16[6144,512]{1,0:T(8,128)(2,1)S(1)} %copy-done, f32[768,4]{1,0:T(8,128)S(1)} %copy.14.gate_q_ref, f32[8,2,2,768]{3,2,1,0:T(2,128)S(1)} %reshape.19.gate_k_ref), custom_call_target="tpu_custom_call" | custom-call | flops 9663676416 | bytes 6291456 | tf_op jit(solution)/shard_map/pallas_call | solution.py:93
  124.3 3.5 all-to-all-start
  127.8 0.0 all-gather.10.cloned.1.call-start
  127.8 0.4 collective-permute-start
  128.2 7.5 %all-to-all-done = bf16[4,192,256]{2,1,0:T(8,128)(2,1)S(1)} async-done(((bf16[4,192,256]{2,1,0:T(8,128)(2,1)}), bf16[4,192,256]{2,1,0:T(8,128)(2,1)S(1)}, u32[]{:S(2)}, u32[]{:S(2)}) %all-to-all-start) | async-done | bytes 393248 | tf_op jit(solution)/shard_map/all_to_all | solution.py:172
  135.8 1.6 fusion
  137.4 0.4 fusion.1
  137.8 0.7 copy-done.3
  138.5 0.4 fusion.7
  138.9 7.6 %collective-permute-done = bf16[256,2048]{1,0:T(8,128)(2,1)} collective-permute-done((bf16[256,2048]{1,0:T(8,128)(2,1)S(1)}, bf16[256,2048]{1,0:T(8,128)(2,1)}, u32[]{:S(2)}, u32[]{:S(2)}) %collective-permute-start) | collective-permute-done | bytes 1048608 | tf_op jit(solution)/shard_map/ppermute | solution.py:116
  146.5 1.8 multiply_reduce_fusion
  148.4 1.1 multiply_convert_fusion.1
  149.4 0.0 all-gather.10.cloned.1.call-update
  149.5 0.0 all-gather.16.cloned.1.call-start
  149.6 7.8 %collective-permute-start.5 = (bf16[688,256]{1,0:T(8,128)(2,1)S(1)}, bf16[688,256]{1,0:T(8,128)(2,1)S(1)}, u32[]{:S(2)}, u32[]{:S(2)}) collective-permute-start(bf16[688,256]{1,0:T(8,128)(2,1)S(1)} %constant_dynamic-slice_fusion), channel_id=1, source_target_pairs={{0,4},{4,0},{1,5},{5,1},{2,6},{6,2},{3,7},{7,3},{8,12},{12,8},{9,1... | collective-permute-start | bytes 1056776 | tf_op jit(solution)/shard_map/ppermute | solution.py:116
  157.4 6.4 %collective-permute-done.5 = bf16[688,256]{1,0:T(8,128)(2,1)S(1)} collective-permute-done((bf16[688,256]{1,0:T(8,128)(2,1)S(1)}, bf16[688,256]{1,0:T(8,128)(2,1)S(1)}, u32[]{:S(2)}, u32[]{:S(2)}) %collective-permute-start.5) | collective-permute-done | bytes 352288 | tf_op jit(solution)/shard_map/ppermute | solution.py:116
  163.8 0.2 broadcast_select_fusion.1
  163.9 0.9 pad_maximum_fusion.3
  164.8 0.0 all-gather.16.cloned.1.call-update
  164.9 0.0 all-gather.14.cloned.1.call-start
  165.0 1.8 collective-permute-start.4
  166.8 5.9 %collective-permute-done.4 = bf16[256,688]{0,1:T(8,128)(2,1)S(1)} collective-permute-done((bf16[256,688]{0,1:T(8,128)(2,1)S(1)}, bf16[256,688]{0,1:T(8,128)(2,1)S(1)}, u32[]{:S(2)}, u32[]{:S(2)}) %collective-permute-start.4) | collective-permute-done | bytes 352288 | tf_op jit(solution)/shard_map/ppermute | solution.py:116
  172.6 0.2 broadcast_select_fusion.3
  172.8 0.9 pad_maximum_fusion.2
  173.7 0.2 reduce-scatter.2.cloned.1.call-start
  174.0 0.0 all-gather.12.cloned.1.call-done
  174.0 73.5 %all-gather.10.cloned.1.call-done = bf16[1536,2048]{1,0:T(8,128)(2,1)} async-done(((bf16[192,2048]{1,0:T(8,128)(2,1)}), bf16[1536,2048]{1,0:T(8,128)(2,1)}) %all-gather.10.cloned.1.call-update) | async-done | bytes 6291472 | tf_op jit(solution)/shard_map/all_gather | solution.py:182
  247.5 10.1 %fusion.17 = f32[1536,688]{0,1:T(8,128)} fusion(bf16[1536,2048]{1,0:T(8,128)(2,1)} %all-gather.10.cloned.1.call-done, bf16[2048,688]{0,1:T(8,128)(2,1)} %all-gather.12.cloned.1.call-done), kind=kOutput, calls=%fused_computation.40 | convolution fusion | flops 4328521728 | bytes 13336576 | tf_op jit(solution)/shard_map/dot_general | solution.py:183
  257.6 49.4 %all-gather.16.cloned.1.call-done = bf16[688,2048]{1,0:T(8,128)(2,1)} async-done(((bf16[688,512]{1,0:T(8,128)(2,1)}), bf16[688,2048]{1,0:T(8,128)(2,1)}) %all-gather.16.cloned.1.call-update) | async-done | bytes 2818064 | tf_op jit(solution)/shard_map/all_gather | solution.py:168
  307.0 58.2 %all-gather.14.cloned.1.call-done = bf16[2048,688]{0,1:T(8,128)(2,1)} async-done(((bf16[512,688]{0,1:T(8,128)(2,1)}), bf16[2048,688]{0,1:T(8,128)(2,1)}) %all-gather.14.cloned.1.call-update) | async-done | bytes 2818064 | tf_op jit(solution)/shard_map/all_gather | solution.py:167
  365.2 18.8 %convolution_convert_fusion = bf16[1536,2048]{1,0:T(8,128)(2,1)} fusion(bf16[688,2048]{1,0:T(8,128)(2,1)} %all-gather.16.cloned.1.call-done, f32[1536,688]{0,1:T(8,128)} %fusion.17, bf16[1536,2048]{1,0:T(8,128)(2,1)} %all-gather.10.cloned.1.call-done, bf16[2048,688]{0,1:T(8,128)(2,1)} %all-gather.14.cloned.1.call-done), kind=kOutput, calls=%fused_computation | convolution fusion | flops 8666529792 | bytes 22446080 | tf_op jit(solution)/shard_map/dot_general | solution.py:186
  384.0 60.6 %reduce-scatter.2.cloned.1.call-done = bf16[192,2048]{1,0:T(8,128)(2,1)} async-done(((bf16[1536,2048]{1,0:T(8,128)(2,1)}), bf16[192,2048]{1,0:T(8,128)(2,1)}) %reduce-scatter.2.cloned.1.call-update) | async-done | bytes 786448 | tf_op jit(solution)/shard_map/reduce_scatter | solution.py:187
  444.6 2.2 add_convert_fusion
  (26 shorter events, 0.2 us)
Async XLA Ops:
  6.5 2.2 copy-start.4
  6.5 105.3 %all-gather.8.cloned.1.call-start = ((), (), s32[]{:S(2)}) async-start(), calls=%async_computation.2 | async-start | bytes 7077888 | tf_op jit(solution)/shard_map/all_gather | solution.py:161
  8.7 165.3 %all-gather.12.cloned.1.call-start = ((), (), s32[]{:S(2)}) async-start(), calls=%async_computation.4 | async-start | bytes 3522560 | tf_op jit(solution)/shard_map/all_gather | solution.py:166
  8.8 11.3 %collective-permute-start.3 = (bf16[256,688]{0,1:T(8,128)(2,1)S(1)}, bf16[256,688]{0,1:T(8,128)(2,1)S(1)}, u32[]{:S(2)}, u32[]{:S(2)}) collective-permute-start(bf16[256,688]{0,1:T(8,128)(2,1)S(1)} %constant_dynamic-slice_fusion.2), channel_id=1, source_target_pairs={{0,4},{4,0},{1,5},{5,1},{2,6},{6,2},{3,7},{7,3},{8,12},{12,8},{9,1... | collective-permute-start | bytes 1056776 | tf_op jit(solution)/shard_map/ppermute | solution.py:116
  11.8 9.4 %copy-start.2 = (bf16[256,2048]{1,0:T(8,128)(2,1)S(1)}, bf16[256,2048]{1,0:T(8,128)(2,1)}, u32[]{:S(2)}) copy-start(bf16[256,2048]{1,0:T(8,128)(2,1)} %param.15) | copy-start | bytes 3145732
  11.8 11.3 %copy-start.7 = (f32[768,4]{0,1:T(4,128)S(1)}, f32[768,4]{0,1:T(4,128)}, u32[]{:S(2)}) copy-start(f32[768,4]{0,1:T(4,128)} %param.14) | copy-start | bytes 36868
  20.2 91.6 %copy-start.1 = (bf16[768,256]{1,0:T(8,128)(2,1)S(1)}, bf16[768,256]{1,0:T(8,128)(2,1)}, u32[]{:S(2)}) copy-start(bf16[768,256]{1,0:T(8,128)(2,1)} %q_ref.1) | copy-start | bytes 1179652
  21.2 114.6 %collective-permute-start.2 = (bf16[256,2048]{1,0:T(8,128)(2,1)S(1)}, bf16[256,2048]{1,0:T(8,128)(2,1)}, u32[]{:S(2)}, u32[]{:S(2)}) collective-permute-start(bf16[256,2048]{1,0:T(8,128)(2,1)S(1)} %copy-done.2), channel_id=1, source_target_pairs={{0,3},{1,0},{2,1},{3,2},{4,7},{5,4},{6,5},{7,6},{8,11},{9,8},{10,9... | collective-permute-start | bytes 3145736 | tf_op jit(solution)/shard_map/ppermute | solution.py:116
  21.6 115.8 %collective-permute-start.1 = (bf16[256,2048]{1,0:T(8,128)(2,1)S(1)}, bf16[256,2048]{1,0:T(8,128)(2,1)S(1)}, u32[]{:S(2)}, u32[]{:S(2)}) collective-permute-start(bf16[256,2048]{1,0:T(8,128)(2,1)S(1)} %copy-done.2), channel_id=1, source_target_pairs={{0,2},{1,3},{2,0},{3,1},{4,6},{5,7},{6,4},{7,5},{8,10},{9,11},{10,... | collective-permute-start | bytes 3145736 | tf_op jit(solution)/shard_map/ppermute | solution.py:116
  111.8 2.8 copy-start
  124.3 11.4 %all-to-all-start = ((bf16[4,192,256]{2,1,0:T(8,128)(2,1)}), bf16[4,192,256]{2,1,0:T(8,128)(2,1)S(1)}, u32[]{:S(2)}, u32[]{:S(2)}) async-start(bf16[4,192,256]{2,1,0:T(8,128)(2,1)} %bitcast.3), calls=%async_computation | async-start | bytes 786432 | tf_op jit(solution)/shard_map/all_to_all | solution.py:172
  127.8 119.8 %all-gather.10.cloned.1.call-start = ((), (), s32[]{:S(2)}) async-start(), calls=%async_computation.3 | async-start | bytes 7077888 | tf_op jit(solution)/shard_map/all_gather | solution.py:182
  127.8 18.7 %collective-permute-start = (bf16[256,2048]{1,0:T(8,128)(2,1)S(1)}, bf16[256,2048]{1,0:T(8,128)(2,1)}, u32[]{:S(2)}, u32[]{:S(2)}) collective-permute-start(bf16[256,2048]{1,0:T(8,128)(2,1)S(1)} %copy-done.2), channel_id=1, source_target_pairs={{0,1},{1,2},{2,3},{3,0},{4,5},{5,6},{6,7},{7,4},{8,9},{9,10},{10,1... | collective-permute-start | bytes 3145736 | tf_op jit(solution)/shard_map/ppermute | solution.py:116
  137.4 1.1 copy-start.3
  138.9 9.4 %copy-start.8 = (f32[2048]{0:T(1024)S(1)}, f32[2048]{0:T(1024)}, u32[]{:S(2)}) copy-start(f32[2048]{0:T(1024)} %param.16) | copy-start | bytes 24580
  148.3 1.2 copy-start.5
  149.5 157.6 %all-gather.16.cloned.1.call-start = ((), (), s32[]{:S(2)}) async-start(), calls=%async_computation.6 | async-start | bytes 3522560 | tf_op jit(solution)/shard_map/all_gather | solution.py:168
  149.6 15.3 %copy-start.6 = (bf16[256,1376]{0,1:T(8,128)(2,1)S(1)}, bf16[256,1376]{0,1:T(8,128)(2,1)}, u32[]{:S(2)}) copy-start(bf16[256,1376]{0,1:T(8,128)(2,1)} %param.18) | copy-start | bytes 2113540
  149.6 14.2 %collective-permute-start.5 = (bf16[688,256]{1,0:T(8,128)(2,1)S(1)}, bf16[688,256]{1,0:T(8,128)(2,1)S(1)}, u32[]{:S(2)}, u32[]{:S(2)}) collective-permute-start(bf16[688,256]{1,0:T(8,128)(2,1)S(1)} %constant_dynamic-slice_fusion), channel_id=1, source_target_pairs={{0,4},{4,0},{1,5},{5,1},{2,6},{6,2},{3,7},{7,3},{8,12},{12,8},{9,1... | collective-permute-start | bytes 1056776 | tf_op jit(solution)/shard_map/ppermute | solution.py:116
  164.9 200.3 %all-gather.14.cloned.1.call-start = ((), (), s32[]{:S(2)}) async-start(), calls=%async_computation.5 | async-start | bytes 3522560 | tf_op jit(solution)/shard_map/all_gather | solution.py:167
  165.0 7.7 %collective-permute-start.4 = (bf16[256,688]{0,1:T(8,128)(2,1)S(1)}, bf16[256,688]{0,1:T(8,128)(2,1)S(1)}, u32[]{:S(2)}, u32[]{:S(2)}) collective-permute-start(bf16[256,688]{0,1:T(8,128)(2,1)S(1)} %constant_dynamic-slice_fusion.1), channel_id=1, source_target_pairs={{0,4},{4,0},{1,5},{5,1},{2,6},{6,2},{3,7},{7,3},{8,12},{12,8},{9,1... | collective-permute-start | bytes 1056776 | tf_op jit(solution)/shard_map/ppermute | solution.py:116
  173.7 270.9 %reduce-scatter.2.cloned.1.call-start = ((), (), s32[]{:S(2)}) async-start(), calls=%async_computation.7 | async-start | bytes 7077888 | tf_op jit(solution)/shard_map/reduce_scatter | solution.py:187
Sparse Core Ops, SparseCore 0:
  9.5 102.2 all-gather.7
  113.4 56.2 all-gather.11
  171.5 75.9 all-gather.9
  249.0 58.0 all-gather.15
  308.4 56.7 all-gather.13
  384.1 60.4 reduce-scatter.1

commit v2 on v1

--- a/solution.py
+++ b/solution.py
@@ -153,7 +153,6 @@
     up_weight,
     down_weight,
 ):
-    rows = queries.shape[0]
     along_x = lax.axis_size("x")
     groups = lax.axis_size("tp")
     shard = lax.axis_index("z") * along_x + lax.axis_index("x")
@@ -163,10 +162,14 @@
     gate_cols = exchange(gate_weight, 1, 0, along_x)
     up_cols = exchange(up_weight, 1, 0, along_x)
     down_rows = exchange(down_weight, 0, 1, along_x)
+    along_z = lax.axis_size("z")
     gate_full = lax.all_gather(gate_cols, "z", axis=0, tiled=True)
     up_full = lax.all_gather(up_cols, "z", axis=0, tiled=True)
-    down_full = lax.all_gather(down_rows, "z", axis=1, tiled=True)
-
+    down_parts = [down_rows] + [shift(down_rows, "z", along_z, d) for d in range(1, along_z)]
+
+    queries, gate_cols, up_cols, down_rows = lax.optimization_barrier(
+        (queries, gate_cols, up_cols, down_rows)
+    )
     attn = flash(shard.astype(jnp.int32), queries, kv_all, cum_gate, gates_all)
 
     own_rows = lax.all_to_all(attn, "tp", split_axis=0, concat_axis=1, tiled=True)
@@ -179,13 +182,28 @@
         mixed = mixed + rounded(
             jnp.dot(part, proj_weights[d], preferred_element_type=jnp.float32)
         )
-    normed_all = lax.all_gather(rms_norm(mixed, norm_gain), ("x", "tp"), axis=0, tiled=True)
+    normed, up_full = lax.optimization_barrier((rms_norm(mixed, norm_gain), up_full))
+    normed_all = lax.all_gather(normed, ("x", "tp"), axis=0, tiled=True)
     gate_sum = jnp.dot(normed_all, gate_full, preferred_element_type=jnp.float32)
     up_sum = jnp.dot(normed_all, up_full, preferred_element_type=jnp.float32)
     hidden = (jax.nn.silu(gate_sum) * up_sum).astype(jnp.bfloat16)
-    ffn_part = jnp.dot(hidden, down_full, preferred_element_type=jnp.float32)
-    ffn = lax.psum_scatter(
-        ffn_part.astype(jnp.bfloat16), ("x", "tp"), scatter_dimension=0, tiled=True
+    ffn_part = jnp.concatenate(
+        [
+            jnp.dot(hidden, part, preferred_element_type=jnp.float32).astype(jnp.bfloat16)
+            for part in down_parts
+        ],
+        axis=1,
+    )
+    turned = lax.psum_scatter(ffn_part, ("x", "tp"), scatter_dimension=0, tiled=True)
+    block = down_parts[0].shape[1]
+    ffn = jnp.concatenate(
+        [
+            lax.dynamic_slice_in_dim(
+                turned, lax.rem(lax.axis_index("z") - c + along_z, along_z) * block, block, 1
+            )
+            for c in range(along_z)
+        ],
+        axis=1,
     ).astype(jnp.float32)
     return (mixed + 0.5 * ffn).astype(jnp.bfloat16)
 
@@ -210,4 +228,5 @@
         P("tp", sp),
     )
     out_specs = P(("z", "x", "tp"), None)
+
     return jax.shard_map(local, mesh=grid, in_specs=in_specs, out_specs=out_specs, check_vma=False)

time: 454 us -> 400 us (0.88)
  waiting for transfers between devices: 334 us -> 246 us
  starting transfers between devices: 18.8 us -> 34.1 us
  blocking collectives: 31.9 us -> 41 us
    all_gather x2 -> x1, waiting for transfers between devices: 123 us -> 47.1 us  [local(): normed_all = lax.all_gather(normed, ('x', 'tp'), axis=0, tiled=True)]
    all_gather x1, waiting for transfers between devices: 0.02 us -> 49.2 us  [local(): gate_full = lax.all_gather(gate_cols, 'z', axis=0, tiled=True)]
    all_gather x1, waiting for transfers between devices: 58.2 us -> 20.3 us  [local(): up_full = lax.all_gather(up_cols, 'z', axis=0, tiled=True)]
    ppermute x6 -> x9, starting transfers between devices: 15 us -> 30.5 us  [shift(): lax.ppermute(value, axis, [(i, (i + step) % size) for i in range(size)])]
    all_gather x1, waiting for transfers between devices: 56.6 us -> 42.1 us  [local(): lax.all_gather(jnp.concatenate([keys, values], axis=1), ('z', 'x'), axis=...]
    ppermute x6 -> x9, waiting for transfers between devices: 28 us -> 15.6 us  [shift(): lax.ppermute(value, axis, [(i, (i + step) % size) for i in range(size)])]
    all_gather x1, blocking collectives: 31.9 us -> 41 us  [local(): gates_all = lax.all_gather(cum_gate.T, ('z', 'x'), axis=0)]
    dot_general x1 -> x5, matrix products: 18.8 us -> 19.3 us  [the longest x1 10.3 us: local(): up_sum = jnp.dot(normed_all, up_full, preferred_element_type=jnp.float32)]
  transfers between devices with their start and end apart: 13 -> 15, of which waited for: 10 -> 8; matrix products, arithmetic and copies ran while one was open for 4% -> 10% of each run, Pallas kernels for 2% -> 2%
where the time goes in v2:
time: 400 us; the launch traced here: 399 us
  waiting for transfers between devices  246 us (62%)
  blocking collectives  41 us (10%)
  matrix products  34.7 us (9%)
  starting transfers between devices  34.1 us (9%)
  between operations  13.4 us (3%)
  other arithmetic  13 us (3%)
  Pallas kernels  9.7 us (2%)
  local copies, waits for them, and re-layouts  6.73 us (2%)
    reduce_scatter x1, waiting for transfers between devices, local(): lax.psum_scatter(ffn_part, ('x', 'tp'), scatter_dimension=0, tiled=True)  64 us
    all_gather x1, waiting for transfers between devices, local(): gate_full = lax.all_gather(gate_cols, 'z', axis=0, tiled=True)  49.2 us
    all_gather x1, waiting for transfers between devices, local(): normed_all = lax.all_gather(normed, ('x', 'tp'), axis=0, tiled=True)  47.1 us
    all_gather x1, waiting for transfers between devices, local(): lax.all_gather(jnp.concatenate([keys, values], axis=1), ('z', 'x'), axis=...  42.1 us
    all_gather x1, blocking collectives, local(): gates_all = lax.all_gather(cum_gate.T, ('z', 'x'), axis=0)  41 us
    ppermute x9, starting transfers between devices, shift(): lax.ppermute(value, axis, [(i, (i + step) % size) for i in range(size)])  30.5 us
    all_gather x1, waiting for transfers between devices, local(): up_full = lax.all_gather(up_cols, 'z', axis=0, tiled=True)  20.3 us
    ppermute x9, waiting for transfers between devices, shift(): lax.ppermute(value, axis, [(i, (i + step) % size) for i in range(size)])  15.6 us
  transfers between devices with their start and end apart: 15, of which 8 were waited for; matrix products, arithmetic and copies ran while one was open for 10% of the time, Pallas kernels for 2%

profile of v2, /device:TPU:0, one launch (start us, length us, event | category | flops | bytes accessed | tf_op | source)
XLA Modules:
  0.0 399.1 jit_solution(1040728563251698295)
XLA Ops:
  6.5 2.2 pad_maximum_fusion.1
  8.7 0.0 all-gather.9.cloned.1.call-start
  8.8 0.8 constant_dynamic-slice_fusion.5
  9.6 3.0 collective-permute-start.1
  12.5 0.8 constant_dynamic-slice_fusion.4
  13.3 8.6 %collective-permute-done.1 = bf16[256,688]{0,1:T(8,128)(2,1)} collective-permute-done((bf16[256,688]{0,1:T(8,128)(2,1)}, bf16[256,688]{0,1:T(8,128)(2,1)}, u32[]{:S(2)}, u32[]{:S(2)}) %collective-permute-start.1) | collective-permute-done | bytes 352288 | tf_op jit(solution)/shard_map/ppermute | solution.py:116
  21.9 1.1 broadcast_select_fusion.3
  23.1 0.9 pad_maximum_fusion.3
  24.0 2.1 collective-permute-start.4
  26.1 0.8 constant_dynamic-slice_fusion.6
  26.9 1.6 collective-permute-start
  28.5 0.2 copy.22.gate_q_ref
  28.7 41.0 %all-gather.1 = f32[8,4,768]{2,1,0:T(4,128)S(1)} all-gather(f32[1,4,768]{2,1,0:T(4,128)S(1)} %bitcast.28), channel_id=2, replica_groups=mesh['z'=4,'x'=2,'tp'=4] {'z','x'}, dimensions={0}, use_global_device_ids=true | all-gather | bytes 110592 | tf_op jit(solution)/shard_map/all_gather | solution.py:159
  69.7 0.1 reshape.19.gate_k_ref
  69.8 0.2 broadcast_select_fusion.1
  69.9 0.9 pad_maximum_fusion.4
  70.9 1.3 broadcast_select_fusion.5
  72.2 0.9 pad_maximum_fusion.2
  73.1 42.1 %all-gather.7.cloned.1.call-done.k_ref.v_ref = bf16[6144,512]{1,0:T(8,128)(2,1)} async-done(((bf16[768,512]{1,0:T(8,128)(2,1)}), bf16[6144,512]{1,0:T(8,128)(2,1)}) %all-gather.7.cloned.1.call-update) | async-done | bytes 6291472 | tf_op jit(solution)/shard_map/all_gather | solution.py:160
  115.2 2.8 copy-done
  118.0 9.7 %shard_map.100 = bf16[768,256]{1,0:T(8,128)(2,1)} custom-call(s32[1]{0:T(128)} %bitcast.shard_ref, bf16[768,256]{1,0:T(8,128)(2,1)S(1)} %copy-done.1, bf16[6144,512]{1,0:T(8,128)(2,1)S(1)} %copy-done, bf16[6144,512]{1,0:T(8,128)(2,1)S(1)} %copy-done, f32[768,4]{1,0:T(8,128)S(1)} %copy.22.gate_q_ref, f32[8,2,2,768]{3,2,1,0:T(2,128)S(1)} %reshape.19.gate_k_ref), custom_call_target="tpu_custom_call" | custom-call | flops 9663676416 | bytes 6291456 | tf_op jit(solution)/shard_map/pallas_call | solution.py:93
  127.7 3.5 all-to-all-start
  131.1 0.0 all-gather.11.cloned.1.call-start
  131.2 0.4 collective-permute-start.3
  131.6 7.5 %all-to-all-done = bf16[4,192,256]{2,1,0:T(8,128)(2,1)S(1)} async-done(((bf16[4,192,256]{2,1,0:T(8,128)(2,1)}), bf16[4,192,256]{2,1,0:T(8,128)(2,1)S(1)}, u32[]{:S(2)}, u32[]{:S(2)}) %all-to-all-start) | async-done | bytes 393248 | tf_op jit(solution)/shard_map/all_to_all | solution.py:175
  139.1 1.6 fusion.1
  140.8 1.7 fusion
  142.5 0.4 fusion.7
  142.9 7.0 %collective-permute-done.3 = bf16[256,2048]{1,0:T(8,128)(2,1)} collective-permute-done((bf16[256,2048]{1,0:T(8,128)(2,1)S(1)}, bf16[256,2048]{1,0:T(8,128)(2,1)}, u32[]{:S(2)}, u32[]{:S(2)}) %collective-permute-start.3) | collective-permute-done | bytes 1048608 | tf_op jit(solution)/shard_map/ppermute | solution.py:116
  149.9 1.9 multiply_reduce_fusion
  151.8 1.1 multiply_convert_fusion.1
  152.9 20.3 %all-gather.9.cloned.1.call-done = bf16[2048,688]{0,1:T(8,128)(2,1)} async-done(((bf16[512,688]{0,1:T(8,128)(2,1)}), bf16[2048,688]{0,1:T(8,128)(2,1)}) %all-gather.9.cloned.1.call-update) | async-done | bytes 2818064 | tf_op jit(solution)/shard_map/all_gather | solution.py:167
  173.2 0.0 all-gather.13.cloned.1.call-start
  173.2 0.5 all-gather.13.cloned.1.call-update
  173.8 0.1 collective-permute-start.6
  173.9 23.3 %collective-permute-start.7 = (bf16[688,512]{1,0:T(8,128)(2,1)S(1)}, bf16[688,512]{1,0:T(8,128)(2,1)}, u32[]{:S(2)}, u32[]{:S(2)}) collective-permute-start(bf16[688,512]{1,0:T(8,128)(2,1)S(1)} %copy-done.7), channel_id=1, source_target_pairs={{0,16},{8,24},{16,0},{24,8},{1,17},{9,25},{17,1},{25,9},{2,18},{10... | collective-permute-start | bytes 2113544 | tf_op jit(solution)/shard_map/ppermute | solution.py:116
  197.2 47.1 %all-gather.11.cloned.1.call-done = bf16[1536,2048]{1,0:T(8,128)(2,1)} async-done(((bf16[192,2048]{1,0:T(8,128)(2,1)}), bf16[1536,2048]{1,0:T(8,128)(2,1)}) %all-gather.11.cloned.1.call-update) | async-done | bytes 6291472 | tf_op jit(solution)/shard_map/all_gather | solution.py:186
  244.3 10.3 %fusion.16 = f32[1536,688]{0,1:T(8,128)} fusion(bf16[1536,2048]{1,0:T(8,128)(2,1)} %all-gather.11.cloned.1.call-done, bf16[2048,688]{0,1:T(8,128)(2,1)} %all-gather.9.cloned.1.call-done), kind=kOutput, calls=%fused_computation.47 | convolution fusion | flops 4328521728 | bytes 13336576 | tf_op jit(solution)/shard_map/dot_general | solution.py:188
  254.6 49.2 %all-gather.13.cloned.1.call-done = bf16[2048,688]{0,1:T(8,128)(2,1)} async-done(((bf16[512,688]{0,1:T(8,128)(2,1)}), bf16[2048,688]{0,1:T(8,128)(2,1)}) %all-gather.13.cloned.1.call-update) | async-done | bytes 2818064 | tf_op jit(solution)/shard_map/all_gather | solution.py:166
  303.8 9.9 %multiply_convert_fusion = bf16[1536,688]{0,1:T(8,128)(2,1)S(1)} fusion(f32[1536,688]{0,1:T(8,128)} %fusion.16, bf16[1536,2048]{1,0:T(8,128)(2,1)} %all-gather.11.cloned.1.call-done, bf16[2048,688]{0,1:T(8,128)(2,1)} %all-gather.13.cloned.1.call-done), kind=kOutput, calls=%fused_computation.1 | convolution fusion | flops 4334862336 | bytes 15450112 | tf_op jit(solution)/shard_map/dot_general | solution.py:187
  313.7 2.5 convolution_convert_fusion.2
  316.2 1.4 convolution_convert_fusion.3
  317.7 2.5 convolution_convert_fusion.1
  320.2 2.5 convolution_convert_fusion
  322.7 3.4 pad_maximum_fusion
  326.1 64.0 %reduce-scatter.2.cloned.1.call-done = bf16[192,2048]{1,0:T(8,128)(2,1)} async-done(((bf16[1536,2048]{1,0:T(8,128)(2,1)}), bf16[192,2048]{1,0:T(8,128)(2,1)}) %reduce-scatter.2.cloned.1.call-update) | async-done | bytes 786448 | tf_op jit(solution)/shard_map/reduce_scatter | solution.py:197
  390.2 1.3 constant_dynamic-slice_fusion.3
  391.4 1.1 add_convert_fusion
  (37 shorter events, 0.2 us)
Async XLA Ops:
  6.5 2.3 copy-start.4
  6.5 6.0 %copy-start.5 = (bf16[1376,256]{1,0:T(8,128)(2,1)S(1)}, bf16[1376,256]{1,0:T(8,128)(2,1)}, u32[]{:S(2)}) copy-start(bf16[1376,256]{1,0:T(8,128)(2,1)} %param.19) | copy-start | bytes 2113540
  6.5 108.6 %all-gather.7.cloned.1.call-start = ((), (), s32[]{:S(2)}) async-start(), calls=%async_computation.2 | async-start | bytes 7077888 | tf_op jit(solution)/shard_map/all_gather | solution.py:160
  8.7 164.4 %all-gather.9.cloned.1.call-start = ((), (), s32[]{:S(2)}) async-start(), calls=%async_computation.3 | async-start | bytes 3522560 | tf_op jit(solution)/shard_map/all_gather | solution.py:167
  9.6 12.4 %collective-permute-start.1 = (bf16[256,688]{0,1:T(8,128)(2,1)}, bf16[256,688]{0,1:T(8,128)(2,1)}, u32[]{:S(2)}, u32[]{:S(2)}) collective-permute-start(bf16[256,688]{0,1:T(8,128)(2,1)} %constant_dynamic-slice_fusion.5), channel_id=1, source_target_pairs={{0,4},{4,0},{1,5},{5,1},{2,6},{6,2},{3,7},{7,3},{8,12},{12,8},{9,1... | collective-permute-start | bytes 1056776 | tf_op jit(solution)/shard_map/ppermute | solution.py:116
  13.3 56.5 %collective-permute-start.2 = (bf16[688,256]{1,0:T(8,128)(2,1)}, bf16[688,256]{1,0:T(8,128)(2,1)S(1)}, u32[]{:S(2)}, u32[]{:S(2)}) collective-permute-start(bf16[688,256]{1,0:T(8,128)(2,1)} %constant_dynamic-slice_fusion.4), channel_id=1, source_target_pairs={{0,4},{4,0},{1,5},{5,1},{2,6},{6,2},{3,7},{7,3},{8,12},{12,8},{9,1... | collective-permute-start | bytes 1056776 | tf_op jit(solution)/shard_map/ppermute | solution.py:116
  13.3 10.7 %copy-start.2 = (bf16[256,2048]{1,0:T(8,128)(2,1)S(1)}, bf16[256,2048]{1,0:T(8,128)(2,1)}, u32[]{:S(2)}) copy-start(bf16[256,2048]{1,0:T(8,128)(2,1)} %param.15) | copy-start | bytes 3145732
  13.3 12.8 %copy-start.6 = (bf16[256,1376]{0,1:T(8,128)(2,1)S(1)}, bf16[256,1376]{0,1:T(8,128)(2,1)}, u32[]{:S(2)}) copy-start(bf16[256,1376]{0,1:T(8,128)(2,1)} %param.17) | copy-start | bytes 2113540
  23.1 5.5 %copy-start.8 = (f32[768,4]{0,1:T(4,128)S(1)}, f32[768,4]{0,1:T(4,128)}, u32[]{:S(2)}) copy-start(f32[768,4]{0,1:T(4,128)} %param.14) | copy-start | bytes 36868
  24.0 115.1 %collective-permute-start.4 = (bf16[256,2048]{1,0:T(8,128)(2,1)S(1)}, bf16[256,2048]{1,0:T(8,128)(2,1)}, u32[]{:S(2)}, u32[]{:S(2)}) collective-permute-start(bf16[256,2048]{1,0:T(8,128)(2,1)S(1)} %copy-done.2), channel_id=1, source_target_pairs={{0,2},{1,3},{2,0},{3,1},{4,6},{5,7},{6,4},{7,5},{8,10},{9,11},{10,... | collective-permute-start | bytes 3145736 | tf_op jit(solution)/shard_map/ppermute | solution.py:116
  26.1 114.7 %collective-permute-start.5 = (bf16[256,2048]{1,0:T(8,128)(2,1)S(1)}, bf16[256,2048]{1,0:T(8,128)(2,1)}, u32[]{:S(2)}, u32[]{:S(2)}) collective-permute-start(bf16[256,2048]{1,0:T(8,128)(2,1)S(1)} %copy-done.2), channel_id=1, source_target_pairs={{0,3},{1,0},{2,1},{3,2},{4,7},{5,4},{6,5},{7,6},{8,11},{9,8},{10,9... | collective-permute-start | bytes 3145736 | tf_op jit(solution)/shard_map/ppermute | solution.py:116
  26.9 44.0 %collective-permute-start = (bf16[256,688]{0,1:T(8,128)(2,1)}, bf16[256,688]{0,1:T(8,128)(2,1)}, u32[]{:S(2)}, u32[]{:S(2)}) collective-permute-start(bf16[256,688]{0,1:T(8,128)(2,1)} %constant_dynamic-slice_fusion.6), channel_id=1, source_target_pairs={{0,4},{4,0},{1,5},{5,1},{2,6},{6,2},{3,7},{7,3},{8,12},{12,8},{9,1... | collective-permute-start | bytes 1056776 | tf_op jit(solution)/shard_map/ppermute | solution.py:116
  70.9 44.3 %copy-start.1 = (bf16[768,256]{1,0:T(8,128)(2,1)S(1)}, bf16[768,256]{1,0:T(8,128)(2,1)}, u32[]{:S(2)}) copy-start(bf16[768,256]{1,0:T(8,128)(2,1)} %q_ref) | copy-start | bytes 1179652
  115.2 2.8 copy-start
  127.7 11.4 %all-to-all-start = ((bf16[4,192,256]{2,1,0:T(8,128)(2,1)}), bf16[4,192,256]{2,1,0:T(8,128)(2,1)S(1)}, u32[]{:S(2)}, u32[]{:S(2)}) async-start(bf16[4,192,256]{2,1,0:T(8,128)(2,1)} %bitcast.3), calls=%async_computation | async-start | bytes 786432 | tf_op jit(solution)/shard_map/all_to_all | solution.py:175
  131.1 113.2 %all-gather.11.cloned.1.call-start = ((), (), s32[]{:S(2)}) async-start(), calls=%async_computation.4 | async-start | bytes 7077888 | tf_op jit(solution)/shard_map/all_gather | solution.py:186
  131.2 18.7 %collective-permute-start.3 = (bf16[256,2048]{1,0:T(8,128)(2,1)S(1)}, bf16[256,2048]{1,0:T(8,128)(2,1)}, u32[]{:S(2)}, u32[]{:S(2)}) collective-permute-start(bf16[256,2048]{1,0:T(8,128)(2,1)S(1)} %copy-done.2), channel_id=1, source_target_pairs={{0,1},{1,2},{2,3},{3,0},{4,5},{5,6},{6,7},{7,4},{8,9},{9,10},{10,1... | collective-permute-start | bytes 3145736 | tf_op jit(solution)/shard_map/ppermute | solution.py:116
  140.8 1.7 copy-start.3
  142.9 8.9 %copy-start.9 = (f32[2048]{0:T(1024)S(1)}, f32[2048]{0:T(1024)}, u32[]{:S(2)}) copy-start(f32[2048]{0:T(1024)} %param.16) | copy-start | bytes 24580
  151.8 22.0 %copy-start.7 = (bf16[688,512]{1,0:T(8,128)(2,1)S(1)}, bf16[688,512]{1,0:T(8,128)(2,1)}, u32[]{:S(2)}) copy-start(bf16[688,512]{1,0:T(8,128)(2,1)} %pad_maximum_fusion.4) | copy-start | bytes 2113540
  173.2 130.6 %all-gather.13.cloned.1.call-start = ((), (), s32[]{:S(2)}) async-start(), calls=%async_computation.5 | async-start | bytes 3522560 | tf_op jit(solution)/shard_map/all_gather | solution.py:166
  173.8 216.4 %reduce-scatter.2.cloned.1.call-start = ((), (), s32[]{:S(2)}) async-start(), calls=%async_computation.6 | async-start | bytes 7077888 | tf_op jit(solution)/shard_map/reduce_scatter | solution.py:197
  173.8 139.9 %collective-permute-start.6 = (bf16[688,512]{1,0:T(8,128)(2,1)S(1)}, bf16[688,512]{1,0:T(8,128)(2,1)}, u32[]{:S(2)}, u32[]{:S(2)}) collective-permute-start(bf16[688,512]{1,0:T(8,128)(2,1)S(1)} %copy-done.7), channel_id=1, source_target_pairs={{0,8},{8,16},{16,24},{24,0},{1,9},{9,17},{17,25},{25,1},{2,10},{10... | collective-permute-start | bytes 2113544 | tf_op jit(solution)/shard_map/ppermute | solution.py:116
  173.9 143.8 %collective-permute-start.7 = (bf16[688,512]{1,0:T(8,128)(2,1)S(1)}, bf16[688,512]{1,0:T(8,128)(2,1)}, u32[]{:S(2)}, u32[]{:S(2)}) collective-permute-start(bf16[688,512]{1,0:T(8,128)(2,1)S(1)} %copy-done.7), channel_id=1, source_target_pairs={{0,16},{8,24},{16,0},{24,8},{1,17},{9,25},{17,1},{25,9},{2,18},{10... | collective-permute-start | bytes 2113544 | tf_op jit(solution)/shard_map/ppermute | solution.py:116
  197.2 123.0 %collective-permute-start.8 = (bf16[688,512]{1,0:T(8,128)(2,1)S(1)}, bf16[688,512]{1,0:T(8,128)(2,1)}, u32[]{:S(2)}, u32[]{:S(2)}) collective-permute-start(bf16[688,512]{1,0:T(8,128)(2,1)S(1)} %copy-done.7), channel_id=1, source_target_pairs={{0,24},{8,0},{16,8},{24,16},{1,25},{9,1},{17,9},{25,17},{2,26},{10... | collective-permute-start | bytes 2113544 | tf_op jit(solution)/shard_map/ppermute | solution.py:116
Sparse Core Ops, SparseCore 0:
  9.5 105.6 all-gather.6
  116.7 56.3 all-gather.8
  175.1 69.1 all-gather.10
  245.7 58.0 all-gather.12
  326.2 63.8 reduce-scatter.1
